TPU v7x, 32 devices: a whole 2x2x4 slice. The times are simulated.
32 devices in a mesh: sp: 4 (over y, core), dp: 8 (over z, x).
Axes of the slice: x: 2, y: 2, z: 4, core: 2. Of those that a mesh axis runs over, the one named last changes fastest.
Arguments:
- query_rows: bfloat16 [8, 512, 4, 128], P('dp', 'sp'), may hold values from -6 to 6
- key_rows: bfloat16 [8, 512, 4, 128], P('dp', 'sp'), may hold values from -6 to 6
- value_rows: bfloat16 [8, 512, 4, 128], P('dp', 'sp'), may hold values from -6 to 6
- map_weight: float32 [4], P('sp'), may hold values from 0.3 to 0.8
- head_gain: float32 [128], replicated, may hold values from 0.1 to 1.9
Outputs:
- mixed: bfloat16 [8, 512, 4, 128], P('dp', 'sp')
All inputs are finite; a program needn't handle non-finite values.
Results may differ from a plain program's by a relative error of at most 0.0049.
Values may be sent and summed in bfloat16 or wider, within the bound.
A program may use at most 64 MiB of HBM per device.

v0:
```python
import math

import jax
import jax.numpy as jnp
from jax import lax
from jax.sharding import PartitionSpec as P

QK = 64
SEGMENT = 64


def map_output(query_map, key_map, value_head):
    length = key_map.shape[0]
    block_len = math.gcd(length, 512)
    key_segment = jnp.arange(length, dtype=jnp.int32) // SEGMENT

    def one_block(start):
        query_block = lax.dynamic_slice_in_dim(query_map, start, block_len, 0)
        query_segment = (start + jnp.arange(block_len, dtype=jnp.int32)) // SEGMENT
        visible = key_segment[None, :] <= query_segment[:, None]
        scores = jnp.dot(query_block, key_map.T, preferred_element_type=jnp.float32) * QK ** (-0.5)
        scores = jnp.where(visible, scores, -jnp.inf)
        scores = scores - jnp.max(scores, axis=-1, keepdims=True)
        raised = jnp.exp(scores)
        weights = raised / jnp.sum(raised, axis=-1, keepdims=True)
        return jnp.dot(weights.astype(jnp.bfloat16), value_head, preferred_element_type=jnp.float32)

    starts = jnp.arange(length // block_len, dtype=jnp.int32) * block_len
    return lax.map(one_block, starts).reshape(length, value_head.shape[1])


def per_heads(query_local, key_local, value_local):
    return lax.map(
        lambda group: map_output(group[0], group[1], group[2]),
        (
            query_local[0].transpose(1, 0, 2),
            key_local[0].transpose(1, 0, 2),
            value_local[0].transpose(1, 0, 2),
        ),
    )


def finish(first_part, second_part, map_weight, head_gain):
    attended = first_part - map_weight[:, None, None] * second_part
    mean_square = jnp.mean(attended * attended, axis=-1, keepdims=True)
    normed = (attended * lax.rsqrt(mean_square + 1e-06) * head_gain).astype(jnp.bfloat16)
    return normed.transpose(1, 0, 2)[None]


def on_device(query_rows, key_rows, value_rows, map_weight, head_gain):
    query_local, key_local, value_local = (
        lax.all_to_all(query_rows, "sp", split_axis=2, concat_axis=1, tiled=True),
        lax.all_to_all(key_rows, "sp", split_axis=2, concat_axis=1, tiled=True),
        lax.all_to_all(value_rows, "sp", split_axis=2, concat_axis=1, tiled=True),
    )
    first_part = per_heads(query_local[..., :QK], key_local[..., :QK], value_local)
    second_part = per_heads(query_local[..., QK:], key_local[..., QK:], value_local)
    normed = finish(first_part, second_part, map_weight, head_gain)
    return lax.all_to_all(normed, "sp", split_axis=1, concat_axis=2, tiled=True)


def solution(mesh):
    return jax.shard_map(
        on_device,
        mesh=mesh,
        in_specs=(
            P("dp", "sp", None, None),
            P("dp", "sp", None, None),
            P("dp", "sp", None, None),
            P("sp"),
            P(),
        ),
        out_specs=P("dp", "sp", None, None),
        check_vma=False,
    )
```

profile of v0, /device:TPU:0, one launch (start us, length us, event | category | flops | bytes accessed | tf_op | source)
XLA Modules:
  0.0 37.9 jit_solution(136135858623358631)
XLA Ops:
  0.0 1.6 %copy.24 = bf16[1,128,4,128]{3,1,0,2:T(8,128)(2,1)} copy(bf16[1,128,4,128]{3,2,1,0:T(4,128)(2,1)} %param.5) | data formatting | bytes 262144 | tf_op args[0]
  1.6 0.0 copy-start
  1.6 4.4 %all-to-all-start = ((bf16[1,128,4,128]{3,1,0,2:T(8,128)(2,1)}), bf16[1,128,4,128]{3,1,0,2:T(8,128)(2,1)S(1)}, u32[]{:S(2)}, u32[]{:S(2)}) async-start(bf16[1,128,4,128]{3,1,0,2:T(8,128)(2,1)} %copy.24), calls=%async_computation | async-start | bytes 262144 | tf_op jit(solution)/shard_map/all_to_all | solution.py:52
  6.0 0.0 copy-done
  6.0 0.0 copy-start.1
  6.0 0.7 %copy.26 = bf16[1,128,4,128]{3,1,0,2:T(8,128)(2,1)} copy(bf16[1,128,4,128]{3,2,1,0:T(4,128)(2,1)S(1)} %copy-done) | data formatting | bytes 262144 | tf_op args[1]
  6.6 0.3 copy-done.1
  6.9 0.7 %copy.28 = bf16[1,128,4,128]{3,1,0,2:T(8,128)(2,1)} copy(bf16[1,128,4,128]{3,2,1,0:T(4,128)(2,1)S(1)} %copy-done.1) | data formatting | bytes 262144 | tf_op args[2]
  8.3 2.3 %all-to-all-done = bf16[1,128,4,128]{3,1,0,2:T(8,128)(2,1)S(1)} async-done(((bf16[1,128,4,128]{3,1,0,2:T(8,128)(2,1)}), bf16[1,128,4,128]{3,1,0,2:T(8,128)(2,1)S(1)}, u32[]{:S(2)}, u32[]{:S(2)}) %all-to-all-start) | async-done | bytes 131104 | tf_op jit(solution)/shard_map/all_to_all | solution.py:52
  10.6 3.3 %all-to-all-start.1 = ((bf16[1,128,4,128]{3,1,0,2:T(8,128)(2,1)}), bf16[1,128,4,128]{3,1,0,2:T(8,128)(2,1)S(1)}, u32[]{:S(2)}, u32[]{:S(2)}) async-start(bf16[1,128,4,128]{3,1,0,2:T(8,128)(2,1)} %copy.26), calls=%async_computation.1 | async-start | bytes 262144 | tf_op jit(solution)/shard_map/all_to_all | solution.py:53
  13.9 4.6 %all-to-all-done.1 = bf16[1,128,4,128]{3,1,0,2:T(8,128)(2,1)S(1)} async-done(((bf16[1,128,4,128]{3,1,0,2:T(8,128)(2,1)}), bf16[1,128,4,128]{3,1,0,2:T(8,128)(2,1)S(1)}, u32[]{:S(2)}, u32[]{:S(2)}) %all-to-all-start.1) | async-done | bytes 131104 | tf_op jit(solution)/shard_map/all_to_all | solution.py:53
  18.5 3.3 %all-to-all-start.2 = ((bf16[1,128,4,128]{3,1,0,2:T(8,128)(2,1)}), bf16[1,128,4,128]{3,1,0,2:T(8,128)(2,1)S(1)}, u32[]{:S(2)}, u32[]{:S(2)}) async-start(bf16[1,128,4,128]{3,1,0,2:T(8,128)(2,1)} %copy.28), calls=%async_computation.2 | async-start | bytes 262144 | tf_op jit(solution)/shard_map/all_to_all | solution.py:54
  21.8 0.4 %fusion.8 = (f32[512]{0:T(512)S(1)}, f32[512,512]{0,1:T(8,128)S(1)}) fusion(bf16[1,512,1,128]{3,1,2,0:T(8,128)(2,1)S(1)} %bitcast.59, bf16[1,512,1,128]{3,1,2,0:T(8,128)(2,1)S(1)} %bitcast.55, s32[512]{0:T(512)S(1)} %add_select_fusion), kind=kOutput, calls=%fused_computation.27 | convolution fusion | flops 34602496 | bytes 1316864 | tf_op jit(solution)/shard_map/while/body/eval_jaxpr/while/body/eval_jaxpr/dot_general | solution.py:21
  22.2 0.3 fusion.9
  22.5 0.2 fusion.3
  22.7 0.2 fusion.2
  22.9 3.5 %all-to-all-done.2 = bf16[1,128,4,128]{3,1,0,2:T(8,128)(2,1)S(1)} async-done(((bf16[1,128,4,128]{3,1,0,2:T(8,128)(2,1)}), bf16[1,128,4,128]{3,1,0,2:T(8,128)(2,1)S(1)}, u32[]{:S(2)}, u32[]{:S(2)}) %all-to-all-start.2) | async-done | bytes 131104 | tf_op jit(solution)/shard_map/all_to_all | solution.py:54
  26.4 0.3 convolution_multiply_fusion.2
  26.7 0.4 multiply_reduce_fusion
  27.1 0.0 copy-start.2
  27.1 0.6 %copy-done.2 = f32[128]{0:T(128)S(1)} copy-done((f32[128]{0:T(128)S(1)}, f32[128]{0:T(128)}, u32[]{:S(2)}) %copy-start.2) | copy-done | bytes 536
  27.8 0.1 fusion.4
  27.8 0.2 copy.31
  28.0 0.5 %broadcast.100 = bf16[]{:T(256)} broadcast(bf16[]{:T(256)} %constant.139), dimensions={} | broadcast | bytes 4
  28.5 1.4 %reduce.2 = bf16[512,128]{1,0:T(8,128)(2,1)S(1)} reduce(bf16[512,1,1,128]{3,2,1,0:T(2,128)(2,1)S(1)} %bitcast.52, bf16[]{:T(256)} %broadcast.100), dimensions={1,2}, to_apply=%bitcast.39.reduce_sub_computation | reduce | bytes 262146
  30.0 7.0 %all_to_all.69 = bf16[4,2,8192]{2,1,0:T(2,128)(2,1)S(1)} all-to-all(bf16[4,2,8192]{2,1,0:T(2,128)(2,1)S(1)} %reshape.64), channel_id=1, replica_groups=mesh['sp'=4,'dp'=8] {'sp'}, dimensions={0} | all-to-all | bytes 262144 | tf_op jit(solution)/shard_map/all_to_all | solution.py:59
  37.0 0.1 reshape.65
  37.1 0.8 %copy.32 = bf16[1,128,4,128]{3,2,1,0:T(4,128)(2,1)} copy(bf16[1,128,4,128]{3,1,2,0:T(8,128)(2,1)S(1)} %bitcast.54) | data formatting | bytes 262144 | tf_op jit(solution)/shard_map/all_to_all | solution.py:59
  (4 shorter events, 0.1 us)
Async XLA Ops:
  1.6 4.4 %copy-start = (bf16[1,128,4,128]{3,2,1,0:T(4,128)(2,1)S(1)}, bf16[1,128,4,128]{3,2,1,0:T(4,128)(2,1)}, u32[]{:S(2)}) copy-start(bf16[1,128,4,128]{3,2,1,0:T(4,128)(2,1)} %param.6) | copy-start | bytes 393220
  1.6 9.0 %all-to-all-start = ((bf16[1,128,4,128]{3,1,0,2:T(8,128)(2,1)}), bf16[1,128,4,128]{3,1,0,2:T(8,128)(2,1)S(1)}, u32[]{:S(2)}, u32[]{:S(2)}) async-start(bf16[1,128,4,128]{3,1,0,2:T(8,128)(2,1)} %copy.24), calls=%async_computation | async-start | bytes 262144 | tf_op jit(solution)/shard_map/all_to_all | solution.py:52
  6.0 1.0 %copy-start.1 = (bf16[1,128,4,128]{3,2,1,0:T(4,128)(2,1)S(1)}, bf16[1,128,4,128]{3,2,1,0:T(4,128)(2,1)}, u32[]{:S(2)}) copy-start(bf16[1,128,4,128]{3,2,1,0:T(4,128)(2,1)} %param.7) | copy-start | bytes 393220
  10.6 7.9 %all-to-all-start.1 = ((bf16[1,128,4,128]{3,1,0,2:T(8,128)(2,1)}), bf16[1,128,4,128]{3,1,0,2:T(8,128)(2,1)S(1)}, u32[]{:S(2)}, u32[]{:S(2)}) async-start(bf16[1,128,4,128]{3,1,0,2:T(8,128)(2,1)} %copy.26), calls=%async_computation.1 | async-start | bytes 262144 | tf_op jit(solution)/shard_map/all_to_all | solution.py:53
  18.5 7.9 %all-to-all-start.2 = ((bf16[1,128,4,128]{3,1,0,2:T(8,128)(2,1)}), bf16[1,128,4,128]{3,1,0,2:T(8,128)(2,1)S(1)}, u32[]{:S(2)}, u32[]{:S(2)}) async-start(bf16[1,128,4,128]{3,1,0,2:T(8,128)(2,1)} %copy.28), calls=%async_computation.2 | async-start | bytes 262144 | tf_op jit(solution)/shard_map/all_to_all | solution.py:54
  27.1 0.7 %copy-start.2 = (f32[128]{0:T(128)S(1)}, f32[128]{0:T(128)}, u32[]{:S(2)}) copy-start(f32[128]{0:T(128)} %param.9) | copy-start | bytes 1540
where the time goes:
time: 38.4 us; the launch traced here: 37.9 us
  starting transfers between devices  11 us (29%)
  waiting for transfers between devices  10.3 us (27%)
  blocking collectives  6.99 us (18%)
  local copies, waits for them, and re-layouts  5.47 us (14%)
  other arithmetic  1.89 us (5%)
  matrix products  1.41 us (4%)
  between operations  0.75 us (2%)
    all_to_all x1, blocking collectives, on_device(): return lax.all_to_all(normed, 'sp', split_axis=1, concat_axis=2, tiled=True)  6.99 us
    all_to_all x1, waiting for transfers between devices, on_device(): lax.all_to_all(key_rows, 'sp', split_axis=2, concat_axis=1, tiled=True)  4.56 us
    unnamed x13, local copies, waits for them, and re-layouts  4.55 us
    all_to_all x1, starting transfers between devices, on_device(): lax.all_to_all(query_rows, 'sp', split_axis=2, concat_axis=1, tiled=True)  4.4 us
    all_to_all x1, waiting for transfers between devices, on_device(): lax.all_to_all(value_rows, 'sp', split_axis=2, concat_axis=1, tiled=True)  3.45 us
    all_to_all x1, starting transfers between devices, on_device(): lax.all_to_all(value_rows, 'sp', split_axis=2, concat_axis=1, tiled=True)  3.33 us
    all_to_all x1, starting transfers between devices, on_device(): lax.all_to_all(key_rows, 'sp', split_axis=2, concat_axis=1, tiled=True)  3.32 us
    all_to_all x1, waiting for transfers between devices, on_device(): lax.all_to_all(query_rows, 'sp', split_axis=2, concat_axis=1, tiled=True)  2.32 us
  transfers between devices with their start and end apart: 3, of which 3 were waited for; matrix products, arithmetic and copies ran while one was open for 6% of the time, Pallas kernels for 0%

commit v1 on v0

v1 whole, which is shorter than its diff:
```python
import functools

import jax
import jax.numpy as jnp
from jax import lax
from jax.experimental import pallas as pl
from jax.experimental.pallas import tpu as pltpu
from jax.sharding import PartitionSpec as P

SEGMENT = 64
CORES = 2
UNROLL = 4
F32 = jnp.float32
BF16 = jnp.bfloat16


def order_matrix(rows, heads, tokens, back):
    out = lax.broadcasted_iota(jnp.int32, (rows, rows), 0)
    src = lax.broadcasted_iota(jnp.int32, (rows, rows), 1)
    if back:
        out, src = src, out
    wanted = (out % tokens) * heads + out // tokens
    return jnp.where(src == wanted, 1.0, 0.0).astype(BF16)


def kernel(
    n, heads, local, qk, hw_ref, gain_ref, q_hbm, k_hbm, v_hbm, out_ref,
    rows_in, staged, gq, gk, gv, made, back, in_sem, send_sem, recv_sem, osend_sem, orecv_sem,
):
    dim = q_hbm.shape[-1]
    mine = heads // n
    me = lax.axis_index("sp")
    tokens = max(16, 256 // heads)
    chunk = tokens * heads

    def there(p):
        return {"sp": p}

    sources = (k_hbm, v_hbm, q_hbm)
    loads = [pltpu.make_async_copy(sources[t], rows_in.at[t], in_sem.at[t]) for t in range(3)]
    for load in loads:
        load.start()
    barrier = pltpu.get_barrier_semaphore()
    for d in range(1, n):
        pl.semaphore_signal(
            barrier, inc=1, device_id=there(lax.rem(me + d, n)),
            device_id_type=pl.DeviceIdType.MESH,
        )
    order = order_matrix(chunk, heads, tokens, False)
    gathered = (gk, gv, gq)
    for t in range(3):
        loads[t].wait()
        for c in range(local // tokens):
            moved = jnp.dot(
                order, rows_in[t, c * chunk:(c + 1) * chunk], preferred_element_type=F32
            ).astype(BF16)
            for h in range(heads):
                staged[t, h, c * tokens:(c + 1) * tokens] = moved[h * tokens:(h + 1) * tokens]
    for t in range(3):
        for g in range(mine):
            gathered[t][g, pl.ds(pl.multiple_of(me * local, local), local)] = staged[t, me * mine + g]
    pl.semaphore_wait(barrier, n - 1)

    here = pl.ds(pl.multiple_of(me * local, local), local)

    def push(t, p):
        return pltpu.make_async_remote_copy(
            src_ref=staged.at[t, pl.ds(p * mine, mine)],
            dst_ref=gathered[t].at[:, here],
            send_sem=send_sem.at[t, p],
            recv_sem=recv_sem.at[t, me],
            device_id=there(p),
            device_id_type=pl.DeviceIdType.MESH,
        )

    base = (me // CORES) * CORES
    peers = [base + lax.rem(me - base + d, CORES) for d in range(1, CORES)]
    peers += [lax.rem(base + d, n) for d in range(CORES, n)]
    for p in peers:
        for t in range(3):
            push(t, p).start()

    def arrive(j):
        @pl.when(me != j)
        def _():
            for t in range(3):
                pltpu.make_async_remote_copy(
                    src_ref=staged.at[t, pl.ds(0, mine)],
                    dst_ref=gathered[t].at[:, pl.ds(pl.multiple_of(j * local, local), local)],
                    send_sem=send_sem.at[t, j],
                    recv_sem=recv_sem.at[t, j],
                    device_id=there(j),
                    device_id_type=pl.DeviceIdType.MESH,
                ).wait_recv()

    def give(i):
        return pltpu.make_async_remote_copy(
            src_ref=made.at[i],
            dst_ref=back.at[pl.ds(me * mine, mine)],
            send_sem=osend_sem.at[i],
            recv_sem=orecv_sem.at[me],
            device_id=there(i),
            device_id_type=pl.DeviceIdType.MESH,
        )

    lower = lax.broadcasted_iota(jnp.int32, (local, dim), 1) < qk
    gain = gain_ref[...]

    def attend(i, width, g):
        start = i * local if isinstance(i, int) else pl.multiple_of(i * local, local)
        query = gq[g, pl.ds(start, local)] * BF16(qk ** -0.5)
        zero = jnp.zeros_like(query)
        both = jnp.concatenate([jnp.where(lower, query, zero), jnp.where(lower, zero, query)], 0)
        scores = lax.dot_general(
            both, gk[g, :width], (((1,), (1,)), ((), ())), preferred_element_type=F32
        )
        row = lax.rem(lax.broadcasted_iota(jnp.int32, scores.shape, 0), local)
        col = lax.broadcasted_iota(jnp.int32, scores.shape, 1)
        visible = col // SEGMENT <= (start + row) // SEGMENT
        scores = jnp.where(visible, scores, -jnp.inf)
        raised = jnp.exp(scores - jnp.max(scores, axis=-1, keepdims=True))
        total = jnp.sum(raised, axis=-1, keepdims=True)
        part = jnp.dot(raised.astype(BF16), gv[g, :width], preferred_element_type=F32)
        part = part / total
        attended = part[:local] - hw_ref[g] * part[local:]
        square = jnp.mean(attended * attended, axis=-1, keepdims=True)
        made[i, g] = (attended * lax.rsqrt(square + 1e-06) * gain).astype(BF16)

    def finish(i):
        @pl.when(me != i)
        def _():
            give(i).start()

        @pl.when(me == i)
        def _():
            for g in range(mine):
                back[me * mine + g] = made[i, g]

    if n <= UNROLL:
        for i in range(n):
            arrive(i)
            for g in range(mine):
                attend(i, (i + 1) * local, g)
            finish(i)
    else:
        for j in range(n):
            arrive(j)

        def body(i, carry):
            for g in range(mine):
                attend(i, n * local, g)
            finish(i)
            return carry

        lax.fori_loop(0, n, body, 0)

    for p in peers:
        pltpu.make_async_remote_copy(
            src_ref=made.at[p],
            dst_ref=back.at[pl.ds(p * mine, mine)],
            send_sem=osend_sem.at[p],
            recv_sem=orecv_sem.at[p],
            device_id=there(p),
            device_id_type=pl.DeviceIdType.MESH,
        ).wait_recv()
    order = order_matrix(chunk, heads, tokens, True)
    for c in range(local // tokens):
        piece = jnp.concatenate(
            [back[h, c * tokens:(c + 1) * tokens] for h in range(heads)], 0
        )
        out_ref[c * chunk:(c + 1) * chunk] = jnp.dot(
            order, piece, preferred_element_type=F32
        ).astype(BF16)
    for p in peers:
        for t in range(3):
            push(t, p).wait_send()
        give(p).wait_send()


def on_device(n, query_rows, key_rows, value_rows, map_weight, head_gain):
    _, local, heads, dim = query_rows.shape
    mine = heads // n
    flat = (local * heads, dim)
    whole = n * local
    out = pl.pallas_call(
        functools.partial(kernel, n, heads, local, dim // 2),
        out_shape=jax.ShapeDtypeStruct(flat, BF16),
        in_specs=[
            pl.BlockSpec(memory_space=pltpu.SMEM),
            pl.BlockSpec(memory_space=pltpu.VMEM),
            pl.BlockSpec(memory_space=pl.ANY),
            pl.BlockSpec(memory_space=pl.ANY),
            pl.BlockSpec(memory_space=pl.ANY),
        ],
        out_specs=pl.BlockSpec(memory_space=pltpu.VMEM),
        scratch_shapes=[
            pltpu.VMEM((3,) + flat, BF16),
            pltpu.VMEM((3, heads, local, dim), BF16),
            pltpu.VMEM((mine, whole, dim), BF16),
            pltpu.VMEM((mine, whole, dim), BF16),
            pltpu.VMEM((mine, whole, dim), BF16),
            pltpu.VMEM((n, mine, local, dim), BF16),
            pltpu.VMEM((heads, local, dim), BF16),
            pltpu.SemaphoreType.DMA((3,)),
            pltpu.SemaphoreType.DMA((3, n)),
            pltpu.SemaphoreType.DMA((3, n)),
            pltpu.SemaphoreType.DMA((n,)),
            pltpu.SemaphoreType.DMA((n,)),
        ],
        compiler_params=pltpu.CompilerParams(collective_id=0, has_side_effects=True),
    )(
        map_weight,
        head_gain.reshape(1, dim),
        query_rows.reshape(flat),
        key_rows.reshape(flat),
        value_rows.reshape(flat),
    )
    return out.reshape(query_rows.shape)


def solution(mesh):
    rows = P("dp", "sp", None, None)
    return jax.shard_map(
        functools.partial(on_device, mesh.shape["sp"]),
        mesh=mesh,
        in_specs=(rows, rows, rows, P("sp"), P()),
        out_specs=rows,
        check_vma=False,
    )
```

time: 38.4 us -> 16.2 us (0.42)
  Pallas kernels: 0 us -> 13.8 us
  starting transfers between devices: 11 us -> 0 us
  waiting for transfers between devices: 10.3 us -> 0 us
  blocking collectives: 6.99 us -> 0 us
  local copies, waits for them, and re-layouts: 5.47 us -> 1.61 us
  other arithmetic: 1.89 us -> 0 us
  matrix products: 1.41 us -> 0 us
    pallas_call x0 -> x1, Pallas kernels: none -> 13.8 us  [on_device(): pl.pallas_call(functools.partial(kernel, n, heads, local, dim // 2), out_...]
    all_to_all x3 -> x0, starting transfers between devices: 11 us -> none  [the longest x1 4.4 us: on_device(): lax.all_to_all(query_rows, 'sp', split_axis=2, concat_axis=1, tiled=True)]
    all_to_all x3 -> x0, waiting for transfers between devices: 10.3 us -> none  [the longest x1 4.56 us: on_device(): lax.all_to_all(key_rows, 'sp', split_axis=2, concat_axis=1, tiled=True)]
    all_to_all x1 -> x0, blocking collectives: 6.99 us -> none  [on_device(): return lax.all_to_all(normed, 'sp', split_axis=1, concat_axis=2, tiled=True)]
    unnamed x13 -> x1, local copies, waits for them, and re-layouts: 4.55 us -> 1.61 us
    dot_general x4 -> x0, matrix products: 1.41 us -> none  [the longest x2 0.71 us: one_block(): jnp.dot(query_block, key_map.T, preferred_element_type=jnp.float32)]
    unnamed x1 -> x0, other arithmetic: 1.41 us -> none
    all_to_all x1 -> x0, local copies, waits for them, and re-layouts: 0.76 us -> none  [on_device(): return lax.all_to_all(normed, 'sp', split_axis=1, concat_axis=2, tiled=True)]
  transfers between devices with their start and end apart: 3 -> 0, of which waited for: 3 -> 0; matrix products, arithmetic and copies ran while one was open for 6% -> 0% of each run, Pallas kernels for 0% -> 0%
where the time goes in v1:
time: 16.2 us; the launch traced here: 16 us
  Pallas kernels  13.8 us (85%)
  local copies, waits for them, and re-layouts  1.61 us (10%)
  between operations  0.66 us (4%)
    pallas_call x1, Pallas kernels, on_device(): pl.pallas_call(functools.partial(kernel, n, heads, local, dim // 2), out_...  13.8 us
    unnamed x1, local copies, waits for them, and re-layouts  1.61 us

profile of v1, /device:TPU:0, one launch (start us, length us, event | category | flops | bytes accessed | tf_op | source)
XLA Modules:
  0.0 16.0 jit_solution(16435956397940024672)
XLA Ops:
  0.7 13.8 %shard_map.55 = bf16[512,128]{1,0:T(8,128)(2,1)} custom-call(f32[1]{0:T(128)S(6)} %copy.7.hw_ref, f32[1,128]{1,0:T(1,128)} %bitcast.9, bf16[512,128]{1,0:T(8,128)(2,1)} %bitcast.6, bf16[512,128]{1,0:T(8,128)(2,1)} %bitcast.7, bf16[512,128]{1,0:T(8,128)(2,1)} %bitcast.8), custom_call_target="tpu_custom_call" | custom-call | tf_op jit(solution)/shard_map/pallas_call | solution.py:185
  14.4 1.6 %copy.8 = bf16[1,128,4,128]{3,2,1,0:T(4,128)(2,1)} copy(bf16[1,128,4,128]{3,2,1,0:T(4,128)(2,1)} %bitcast.5) | data formatting | bytes 262144

commit v2 on v1

--- a/solution.py
+++ b/solution.py
@@ -10,6 +10,7 @@
 SEGMENT = 64
 CORES = 2
 UNROLL = 4
+KERNEL_BYTES = 32 * 1024 * 1024
 F32 = jnp.float32
 BF16 = jnp.bfloat16
 
@@ -24,8 +25,8 @@
 
 
 def kernel(
-    n, heads, local, qk, hw_ref, gain_ref, q_hbm, k_hbm, v_hbm, out_ref,
-    rows_in, staged, gq, gk, gv, made, back, in_sem, send_sem, recv_sem, osend_sem, orecv_sem,
+    n, heads, local, qk, hw_ref, gain_hbm, q_hbm, k_hbm, v_hbm, back,
+    rows_in, staged, gq, gk, gv, made, gain_ref, in_sem, send_sem, recv_sem, osend_sem, orecv_sem,
 ):
     dim = q_hbm.shape[-1]
     mine = heads // n
@@ -38,6 +39,7 @@
 
     sources = (k_hbm, v_hbm, q_hbm)
     loads = [pltpu.make_async_copy(sources[t], rows_in.at[t], in_sem.at[t]) for t in range(3)]
+    loads.append(pltpu.make_async_copy(gain_hbm, gain_ref, in_sem.at[3]))
     for load in loads:
         load.start()
     barrier = pltpu.get_barrier_semaphore()
@@ -48,6 +50,21 @@
         )
     order = order_matrix(chunk, heads, tokens, False)
     gathered = (gk, gv, gq)
+    here = pl.ds(pl.multiple_of(me * local, local), local)
+
+    def push(t, p):
+        return pltpu.make_async_remote_copy(
+            src_ref=staged.at[t, pl.ds(p * mine, mine)],
+            dst_ref=gathered[t].at[:, here],
+            send_sem=send_sem.at[t, p],
+            recv_sem=recv_sem.at[t, me],
+            device_id=there(p),
+            device_id_type=pl.DeviceIdType.MESH,
+        )
+
+    base = (me // CORES) * CORES
+    peers = [lax.rem(base + d, n) for d in range(CORES, n)]
+    peers += [base + lax.rem(me - base + d, CORES) for d in range(1, CORES)]
     for t in range(3):
         loads[t].wait()
         for c in range(local // tokens):
@@ -56,29 +73,17 @@
             ).astype(BF16)
             for h in range(heads):
                 staged[t, h, c * tokens:(c + 1) * tokens] = moved[h * tokens:(h + 1) * tokens]
+        if t == 0:
+            pl.semaphore_wait(barrier, n - 1)
+        push(t, peers[0]).start()
+        for p in peers[n - CORES:]:
+            push(t, p).start()
+    for p in peers[1:n - CORES]:
+        for t in range(3):
+            push(t, p).start()
     for t in range(3):
         for g in range(mine):
-            gathered[t][g, pl.ds(pl.multiple_of(me * local, local), local)] = staged[t, me * mine + g]
-    pl.semaphore_wait(barrier, n - 1)
-
-    here = pl.ds(pl.multiple_of(me * local, local), local)
-
-    def push(t, p):
-        return pltpu.make_async_remote_copy(
-            src_ref=staged.at[t, pl.ds(p * mine, mine)],
-            dst_ref=gathered[t].at[:, here],
-            send_sem=send_sem.at[t, p],
-            recv_sem=recv_sem.at[t, me],
-            device_id=there(p),
-            device_id_type=pl.DeviceIdType.MESH,
-        )
-
-    base = (me // CORES) * CORES
-    peers = [base + lax.rem(me - base + d, CORES) for d in range(1, CORES)]
-    peers += [lax.rem(base + d, n) for d in range(CORES, n)]
-    for p in peers:
-        for t in range(3):
-            push(t, p).start()
+            gathered[t][g, here] = staged[t, me * mine + g]
 
     def arrive(j):
         @pl.when(me != j)
@@ -104,6 +109,7 @@
         )
 
     lower = lax.broadcasted_iota(jnp.int32, (local, dim), 1) < qk
+    loads[3].wait()
     gain = gain_ref[...]
 
     def attend(i, width, g):
@@ -163,18 +169,23 @@
             device_id=there(p),
             device_id_type=pl.DeviceIdType.MESH,
         ).wait_recv()
-    order = order_matrix(chunk, heads, tokens, True)
-    for c in range(local // tokens):
-        piece = jnp.concatenate(
-            [back[h, c * tokens:(c + 1) * tokens] for h in range(heads)], 0
-        )
-        out_ref[c * chunk:(c + 1) * chunk] = jnp.dot(
-            order, piece, preferred_element_type=F32
-        ).astype(BF16)
     for p in peers:
         for t in range(3):
             push(t, p).wait_send()
         give(p).wait_send()
+
+
+def interleave(heads, local, back_ref, out_ref):
+    tokens = max(16, 256 // heads)
+    chunk = tokens * heads
+    order = order_matrix(chunk, heads, tokens, True)
+    for c in range(local // tokens):
+        piece = jnp.concatenate(
+            [back_ref[h, c * tokens:(c + 1) * tokens] for h in range(heads)], 0
+        )
+        out_ref[c * chunk:(c + 1) * chunk] = jnp.dot(
+            order, piece, preferred_element_type=F32
+        ).astype(BF16)
 
 
 def on_device(n, query_rows, key_rows, value_rows, map_weight, head_gain):
@@ -184,14 +195,9 @@
     whole = n * local
     out = pl.pallas_call(
         functools.partial(kernel, n, heads, local, dim // 2),
-        out_shape=jax.ShapeDtypeStruct(flat, BF16),
-        in_specs=[
-            pl.BlockSpec(memory_space=pltpu.SMEM),
-            pl.BlockSpec(memory_space=pltpu.VMEM),
-            pl.BlockSpec(memory_space=pl.ANY),
-            pl.BlockSpec(memory_space=pl.ANY),
-            pl.BlockSpec(memory_space=pl.ANY),
-        ],
+        out_shape=pltpu.VMEM((heads, local, dim), BF16),
+        in_specs=[pl.BlockSpec(memory_space=pltpu.SMEM)]
+        + [pl.BlockSpec(memory_space=pltpu.HBM)] * 4,
         out_specs=pl.BlockSpec(memory_space=pltpu.VMEM),
         scratch_shapes=[
             pltpu.VMEM((3,) + flat, BF16),
@@ -200,8 +206,8 @@
             pltpu.VMEM((mine, whole, dim), BF16),
             pltpu.VMEM((mine, whole, dim), BF16),
             pltpu.VMEM((n, mine, local, dim), BF16),
-            pltpu.VMEM((heads, local, dim), BF16),
-            pltpu.SemaphoreType.DMA((3,)),
+            pltpu.VMEM((1, dim), F32),
+            pltpu.SemaphoreType.DMA((4,)),
             pltpu.SemaphoreType.DMA((3, n)),
             pltpu.SemaphoreType.DMA((3, n)),
             pltpu.SemaphoreType.DMA((n,)),
@@ -215,7 +221,14 @@
         key_rows.reshape(flat),
         value_rows.reshape(flat),
     )
-    return out.reshape(query_rows.shape)
+    rows = pl.pallas_call(
+        functools.partial(interleave, heads, local),
+        out_shape=jax.ShapeDtypeStruct(flat, BF16),
+        in_specs=[pl.BlockSpec(memory_space=pltpu.VMEM)],
+        out_specs=pl.BlockSpec(memory_space=pltpu.VMEM),
+        compiler_params=pltpu.CompilerParams(vmem_limit_bytes=KERNEL_BYTES),
+    )(out)
+    return rows.reshape(query_rows.shape)
 
 
 def solution(mesh):

time: 16.2 us -> 14 us (0.86)
  local copies, waits for them, and re-layouts: 1.61 us -> 0 us
  Pallas kernels: 13.8 us -> 13.2 us
    unnamed x1 -> x0, local copies, waits for them, and re-layouts: 1.61 us -> none
    pallas_call x1, Pallas kernels: 13.8 us -> 12.3 us  [on_device(): pl.pallas_call(functools.partial(kernel, n, heads, local, dim // 2), out_...]
    pallas_call x0 -> x1, Pallas kernels: none -> 0.87 us  [on_device(): pl.pallas_call(functools.partial(interleave, heads, local), out_shape=jax...]
where the time goes in v2:
time: 14 us; the launch traced here: 13.8 us
  Pallas kernels  13.2 us (94%)
  between operations  0.66 us (5%)
    pallas_call x1, Pallas kernels, on_device(): pl.pallas_call(functools.partial(kernel, n, heads, local, dim // 2), out_...  12.3 us
    pallas_call x1, Pallas kernels, on_device(): pl.pallas_call(functools.partial(interleave, heads, local), out_shape=jax...  0.87 us

profile of v2, /device:TPU:0, one launch (start us, length us, event | category | flops | bytes accessed | tf_op | source)
XLA Modules:
  0.0 13.8 jit_solution(6887870272130340722)
XLA Ops:
  0.7 12.3 %shard_map.55.back_ref = bf16[4,128,128]{2,1,0:T(8,128)(2,1)S(1)} custom-call(f32[1]{0:T(128)S(6)} %copy.6.hw_ref, f32[1,128]{1,0:T(1,128)} %bitcast.8, bf16[512,128]{1,0:T(8,128)(2,1)} %bitcast.5, bf16[512,128]{1,0:T(8,128)(2,1)} %bitcast.6, bf16[512,128]{1,0:T(8,128)(2,1)} %bitcast.7), custom_call_target="tpu_custom_call" | custom-call | tf_op jit(solution)/shard_map/pallas_call | solution.py:196
  12.9 0.9 %shard_map.56 = bf16[512,128]{1,0:T(8,128)(2,1)} custom-call(bf16[4,128,128]{2,1,0:T(8,128)(2,1)S(1)} %shard_map.55.back_ref), custom_call_target="tpu_custom_call" | custom-call | tf_op jit(solution)/shard_map/pallas_call | solution.py:224

commit v3 on v2

--- a/solution.py
+++ b/solution.py
@@ -175,6 +175,220 @@
         give(p).wait_send()
 
 
+def pair_kernel(
+    heads, local, qk, hw_ref, gain_hbm, q_hbm, k_hbm, v_hbm, back,
+    rows_in, gq, gk, gv, lent, made, gain_ref, weight, in_sem, wsend_sem, wrecv_sem,
+    send_sem, recv_sem, qsend_sem, qrecv_sem, osend_sem, orecv_sem,
+):
+    dim = q_hbm.shape[-1]
+    moved = heads // 4
+    me = lax.axis_index("sp")
+    tokens = max(16, 256 // heads)
+    chunk = tokens * heads
+    across = lax.rem(me + CORES, 2 * CORES)
+    beside = me + 1 - 2 * lax.rem(me, CORES)
+    gathered = (gk, gv)
+
+    loads = [
+        pltpu.make_async_copy(src, rows_in.at[t], in_sem.at[t])
+        for t, src in enumerate((k_hbm, v_hbm, q_hbm))
+    ]
+    loads.append(pltpu.make_async_copy(gain_hbm, gain_ref, in_sem.at[3]))
+    for load in loads:
+        load.start()
+    barrier = pltpu.get_barrier_semaphore()
+    others = [lax.rem(me + d, 2 * CORES) for d in range(1, 2 * CORES)]
+    for p in others:
+        pl.semaphore_signal(
+            barrier, inc=1, device_id={"sp": p}, device_id_type=pl.DeviceIdType.MESH
+        )
+    mine = heads // (2 * CORES)
+    for g in range(mine):
+        weight[me * mine + g] = jnp.full((8, dim), hw_ref[g], F32)
+
+    def tell(p, j):
+        rows = weight.at[pl.ds(j * mine, mine)]
+        return pltpu.make_async_remote_copy(
+            src_ref=rows, dst_ref=rows,
+            send_sem=wsend_sem.at[p], recv_sem=wrecv_sem.at[j],
+            device_id={"sp": p}, device_id_type=pl.DeviceIdType.MESH,
+        )
+
+    order = order_matrix(chunk, heads, tokens, False)
+
+    def relay(t):
+        loads[t].wait()
+        for c in range(local // tokens):
+            rows = jnp.dot(
+                order, rows_in[t, c * chunk:(c + 1) * chunk], preferred_element_type=F32
+            ).astype(BF16)
+            for h in range(heads):
+                piece = rows[h * tokens:(h + 1) * tokens]
+                if t == 2:
+                    gq[h, c * tokens:(c + 1) * tokens] = piece
+                else:
+                    start = pl.multiple_of(me * local + c * tokens, tokens)
+                    gathered[t][h, pl.ds(start, tokens)] = piece
+
+    def block(t, h, j):
+        start = j * local if isinstance(j, int) else pl.multiple_of(j * local, local)
+        return gathered[t].at[h, pl.ds(start, local)]
+
+    def move(t, h, j, p, kind):
+        return pltpu.make_async_remote_copy(
+            src_ref=block(t, h, j),
+            dst_ref=block(t, h, j),
+            send_sem=send_sem.at[kind, t, h, j],
+            recv_sem=recv_sem.at[t, h, j],
+            device_id={"sp": p},
+            device_id_type=pl.DeviceIdType.MESH,
+        )
+
+    def lend(h, p):
+        return pltpu.make_async_remote_copy(
+            src_ref=gq.at[h], dst_ref=lent.at[h],
+            send_sem=qsend_sem.at[h], recv_sem=qrecv_sem.at[h],
+            device_id={"sp": p}, device_id_type=pl.DeviceIdType.MESH,
+        )
+
+    def give(h, p):
+        return pltpu.make_async_remote_copy(
+            src_ref=made.at[h], dst_ref=back.at[h],
+            send_sem=osend_sem.at[h], recv_sem=orecv_sem.at[h],
+            device_id={"sp": p}, device_id_type=pl.DeviceIdType.MESH,
+        )
+
+    relay(0)
+    pl.semaphore_wait(barrier, 2 * CORES - 1)
+    for p in others:
+        tell(p, me).start()
+
+    @pl.when(me < CORES)
+    def _():
+        move(0, moved, me, across, 0).start()
+
+    @pl.when(me >= CORES)
+    def _():
+        move(0, 0, me, across, 0).start()
+
+    relay(1)
+    relay(2)
+    loads[3].wait()
+    gain = gain_ref[...]
+    lower = lax.broadcasted_iota(jnp.int32, (local, dim), 1) < qk
+    row = lax.rem(lax.broadcasted_iota(jnp.int32, (2 * local, local), 0), local)
+    col = lax.broadcasted_iota(jnp.int32, (2 * local, local), 1)
+    visible = col // SEGMENT <= row // SEGMENT
+
+    def weigh(query, h, i):
+        query = query * BF16(qk ** -0.5)
+        zero = jnp.zeros_like(query)
+        both = jnp.concatenate([jnp.where(lower, query, zero), jnp.where(lower, zero, query)], 0)
+        across_dim = (((1,), (1,)), ((), ()))
+        scores = lax.dot_general(
+            both, gk[h, i * local:(i + 1) * local], across_dim, preferred_element_type=F32
+        )
+        scores = jnp.where(visible, scores, -jnp.inf)
+        if i:
+            past = lax.dot_general(
+                both, gk[h, :i * local], across_dim, preferred_element_type=F32
+            )
+            scores = jnp.concatenate([past, scores], 1)
+        raised = jnp.exp(scores - jnp.max(scores, axis=-1, keepdims=True))
+        return raised.astype(BF16), jnp.sum(raised, axis=-1, keepdims=True)
+
+    def mix(raised, total, h, i):
+        part = jnp.dot(raised, gv[h, :(i + 1) * local], preferred_element_type=F32)
+        part = part / total
+        attended = part[:local] - weight[h, 0:1] * part[local:]
+        square = jnp.mean(attended * attended, axis=-1, keepdims=True)
+        return (attended * lax.rsqrt(square + 1e-06) * gain).astype(BF16)
+
+    def role(r):
+        side, other = r + 1 - 2 * (r % CORES), (r + CORES) % (2 * CORES)
+        sent = []
+
+        def go(copy, begun=False):
+            if not begun:
+                copy.start()
+            sent.append(copy)
+
+        def hear():
+            for p in range(2 * CORES):
+                if p != r:
+                    tell(p, p).wait_recv()
+
+        def landed(t, h, j):
+            move(t, h, j, side, 1).wait_recv()
+
+        def pass_on(t, h, j):
+            landed(t, h, j)
+            go(move(t, h, j, side, 1))
+
+        if r < CORES:
+            for h in range(moved, heads):
+                for t in range(2):
+                    go(move(t, h, r, other, 0), begun=(h == moved and t == 0))
+            for h in range(heads if r == 0 else moved):
+                for t in range(2):
+                    go(move(t, h, r, side, 1))
+            hear()
+            for h in range(heads):
+                if r:
+                    landed(0, h, 0)
+                    landed(1, h, 0)
+                back[h] = mix(*weigh(gq[h], h, r), h, r)
+            for h in range(moved):
+                if r == 0:
+                    pass_on(0, h, other)
+                    pass_on(1, h, other)
+                    landed(0, h, 1)
+                    landed(1, h, 1)
+                else:
+                    landed(0, h, other)
+                    landed(0, h, other - 1)
+                lend(h, other).wait_recv()
+                weights = weigh(lent[h], h, other)
+                if r:
+                    landed(1, h, other)
+                    landed(1, h, other - 1)
+                made[h] = mix(*weights, h, other)
+                go(give(h, other))
+        else:
+            for h in range(moved):
+                for t in range(2):
+                    go(move(t, h, r, other, 0), begun=(h == 0 and t == 0))
+                go(lend(h, other))
+            if r == CORES:
+                for h in range(moved, heads):
+                    for t in range(2):
+                        go(move(t, h, r, side, 1))
+            hear()
+            far = side - CORES
+            pass_on(0, moved, other)
+            for h in range(moved, heads):
+                pass_on(1, h, other)
+                if h + 1 < heads:
+                    pass_on(0, h + 1, other)
+                landed(0, h, far)
+                if r > CORES:
+                    landed(0, h, side)
+                weights = weigh(gq[h], h, r)
+                landed(1, h, far)
+                if r > CORES:
+                    landed(1, h, side)
+                back[h] = mix(*weights, h, r)
+            for h in range(moved):
+                give(h, other).wait_recv()
+        for copy in sent:
+            copy.wait_send()
+
+    for r in range(2 * CORES):
+        pl.when(me == r)(functools.partial(role, r))
+    for p in others:
+        tell(p, me).wait_send()
+
+
 def interleave(heads, local, back_ref, out_ref):
     tokens = max(16, 256 // heads)
     chunk = tokens * heads
@@ -193,14 +407,27 @@
     mine = heads // n
     flat = (local * heads, dim)
     whole = n * local
-    out = pl.pallas_call(
-        functools.partial(kernel, n, heads, local, dim // 2),
-        out_shape=pltpu.VMEM((heads, local, dim), BF16),
-        in_specs=[pl.BlockSpec(memory_space=pltpu.SMEM)]
-        + [pl.BlockSpec(memory_space=pltpu.HBM)] * 4,
-        out_specs=pl.BlockSpec(memory_space=pltpu.VMEM),
-        scratch_shapes=[
-            pltpu.VMEM((3,) + flat, BF16),
+    paired = n == 2 * CORES and heads % 4 == 0
+    if paired:
+        moved = heads // 4
+        body = functools.partial(pair_kernel, heads, local, dim // 2)
+        scratch = [
+            pltpu.VMEM((heads, local, dim), BF16),
+            pltpu.VMEM((heads, whole, dim), BF16),
+            pltpu.VMEM((heads, whole, dim), BF16),
+            pltpu.VMEM((moved, local, dim), BF16),
+            pltpu.VMEM((moved, local, dim), BF16),
+            pltpu.VMEM((1, dim), F32),
+            pltpu.VMEM((heads, 8, dim), F32),
+            pltpu.SemaphoreType.DMA((4,)),
+            pltpu.SemaphoreType.DMA((n,)),
+            pltpu.SemaphoreType.DMA((n,)),
+            pltpu.SemaphoreType.DMA((2, 2, heads, n)),
+            pltpu.SemaphoreType.DMA((2, heads, n)),
+        ] + [pltpu.SemaphoreType.DMA((moved,))] * 4
+    else:
+        body = functools.partial(kernel, n, heads, local, dim // 2)
+        scratch = [
             pltpu.VMEM((3, heads, local, dim), BF16),
             pltpu.VMEM((mine, whole, dim), BF16),
             pltpu.VMEM((mine, whole, dim), BF16),
@@ -212,7 +439,14 @@
             pltpu.SemaphoreType.DMA((3, n)),
             pltpu.SemaphoreType.DMA((n,)),
             pltpu.SemaphoreType.DMA((n,)),
-        ],
+        ]
+    out = pl.pallas_call(
+        body,
+        out_shape=pltpu.VMEM((heads, local, dim), BF16),
+        in_specs=[pl.BlockSpec(memory_space=pltpu.SMEM)]
+        + [pl.BlockSpec(memory_space=pltpu.HBM)] * 4,
+        out_specs=pl.BlockSpec(memory_space=pltpu.VMEM),
+        scratch_shapes=[pltpu.VMEM((3,) + flat, BF16)] + scratch,
         compiler_params=pltpu.CompilerParams(collective_id=0, has_side_effects=True),
     )(
         map_weight,

time: 14 us -> 12.2 us (0.87)
  the two profiles are of different devices: /device:TPU:0 before, /device:TPU:21 now
where the time goes in v3:
time: 12.2 us; the launch traced here: 12 us
  Pallas kernels  11.4 us (93%)
  between operations  0.66 us (5%)
    pallas_call x1, Pallas kernels, on_device(): pl.pallas_call(body, out_shape=pltpu.VMEM((heads, local, dim), BF16), in_...  10.5 us
    pallas_call x1, Pallas kernels, on_device(): pl.pallas_call(functools.partial(interleave, heads, local), out_shape=jax...  0.87 us

profile of v3, /device:TPU:21, one launch (start us, length us, event | category | flops | bytes accessed | tf_op | source)
XLA Modules:
  0.0 12.0 jit_solution(7561547448961879466)
XLA Ops:
  0.7 10.5 %shard_map.55.back_ref = bf16[4,128,128]{2,1,0:T(8,128)(2,1)S(1)} custom-call(f32[1]{0:T(128)S(6)} %copy.6.hw_ref, f32[1,128]{1,0:T(1,128)} %bitcast.8, bf16[512,128]{1,0:T(8,128)(2,1)} %bitcast.5, bf16[512,128]{1,0:T(8,128)(2,1)} %bitcast.6, bf16[512,128]{1,0:T(8,128)(2,1)} %bitcast.7), custom_call_target="tpu_custom_call" | custom-call | tf_op jit(solution)/shard_map/pallas_call | solution.py:443
  11.2 0.9 %shard_map.56 = bf16[512,128]{1,0:T(8,128)(2,1)} custom-call(bf16[4,128,128]{2,1,0:T(8,128)(2,1)S(1)} %shard_map.55.back_ref), custom_call_target="tpu_custom_call" | custom-call | tf_op jit(solution)/shard_map/pallas_call | solution.py:458

commit v4 on v3

--- a/solution.py
+++ b/solution.py
@@ -185,7 +185,7 @@
     me = lax.axis_index("sp")
     tokens = max(16, 256 // heads)
     chunk = tokens * heads
-    across = lax.rem(me + CORES, 2 * CORES)
+    across = 2 * CORES - 1 - me
     beside = me + 1 - 2 * lax.rem(me, CORES)
     gathered = (gk, gv)
 
@@ -305,7 +305,7 @@
         return (attended * lax.rsqrt(square + 1e-06) * gain).astype(BF16)
 
     def role(r):
-        side, other = r + 1 - 2 * (r % CORES), (r + CORES) % (2 * CORES)
+        side, other = r + 1 - 2 * (r % CORES), 2 * CORES - 1 - r
         sent = []
 
         def go(copy, begun=False):
@@ -339,19 +339,19 @@
                     landed(1, h, 0)
                 back[h] = mix(*weigh(gq[h], h, r), h, r)
             for h in range(moved):
-                if r == 0:
+                if r:
                     pass_on(0, h, other)
                     pass_on(1, h, other)
+                else:
                     landed(0, h, 1)
                     landed(1, h, 1)
-                else:
+                    landed(0, h, other - 1)
                     landed(0, h, other)
-                    landed(0, h, other - 1)
                 lend(h, other).wait_recv()
                 weights = weigh(lent[h], h, other)
-                if r:
+                if r == 0:
+                    landed(1, h, other - 1)
                     landed(1, h, other)
-                    landed(1, h, other - 1)
                 made[h] = mix(*weights, h, other)
                 go(give(h, other))
         else:
@@ -364,7 +364,7 @@
                     for t in range(2):
                         go(move(t, h, r, side, 1))
             hear()
-            far = side - CORES
+            far = CORES - 1 - other
             pass_on(0, moved, other)
             for h in range(moved, heads):
                 pass_on(1, h, other)

time: 12.2 us -> 13.9 us (1.14)
  the two profiles are of different devices: /device:TPU:21 before, /device:TPU:0 now
where the time goes in v4:
time: 13.9 us; the launch traced here: 13.7 us
  Pallas kernels  13.1 us (94%)
  between operations  0.66 us (5%)
    pallas_call x1, Pallas kernels, on_device(): pl.pallas_call(body, out_shape=pltpu.VMEM((heads, local, dim), BF16), in_...  12.2 us
    pallas_call x1, Pallas kernels, on_device(): pl.pallas_call(functools.partial(interleave, heads, local), out_shape=jax...  0.87 us

profile of v4, /device:TPU:0, one launch (start us, length us, event | category | flops | bytes accessed | tf_op | source)
XLA Modules:
  0.0 13.7 jit_solution(9670778361222121543)
XLA Ops:
  0.7 12.2 %shard_map.55.back_ref = bf16[4,128,128]{2,1,0:T(8,128)(2,1)S(1)} custom-call(f32[1]{0:T(128)S(6)} %copy.6.hw_ref, f32[1,128]{1,0:T(1,128)} %bitcast.8, bf16[512,128]{1,0:T(8,128)(2,1)} %bitcast.5, bf16[512,128]{1,0:T(8,128)(2,1)} %bitcast.6, bf16[512,128]{1,0:T(8,128)(2,1)} %bitcast.7), custom_call_target="tpu_custom_call" | custom-call | tf_op jit(solution)/shard_map/pallas_call | solution.py:443
  12.8 0.9 %shard_map.56 = bf16[512,128]{1,0:T(8,128)(2,1)} custom-call(bf16[4,128,128]{2,1,0:T(8,128)(2,1)S(1)} %shard_map.55.back_ref), custom_call_target="tpu_custom_call" | custom-call | tf_op jit(solution)/shard_map/pallas_call | solution.py:458

commit v5 on v3

--- a/solution.py
+++ b/solution.py
@@ -204,7 +204,7 @@
         )
     mine = heads // (2 * CORES)
     for g in range(mine):
-        weight[me * mine + g] = jnp.full((8, dim), hw_ref[g], F32)
+        weight[me * mine + g] = jnp.full((1, dim), hw_ref[g], F32)
 
     def tell(p, j):
         rows = weight.at[pl.ds(j * mine, mine)]
@@ -297,10 +297,18 @@
         raised = jnp.exp(scores - jnp.max(scores, axis=-1, keepdims=True))
         return raised.astype(BF16), jnp.sum(raised, axis=-1, keepdims=True)
 
-    def mix(raised, total, h, i):
-        part = jnp.dot(raised, gv[h, :(i + 1) * local], preferred_element_type=F32)
+    def mix(raised, total, h, i, late=None, wait=None):
+        if late is None:
+            part = jnp.dot(raised, gv[h, :(i + 1) * local], preferred_element_type=F32)
+        else:
+            part = 0.0
+            for j in [j for j in range(i + 1) if j != late] + [late]:
+                if j == late:
+                    wait()
+                at = slice(j * local, (j + 1) * local)
+                part += jnp.dot(raised[:, at], gv[h, at], preferred_element_type=F32)
         part = part / total
-        attended = part[:local] - weight[h, 0:1] * part[local:]
+        attended = part[:local] - weight[h] * part[local:]
         square = jnp.mean(attended * attended, axis=-1, keepdims=True)
         return (attended * lax.rsqrt(square + 1e-06) * gain).astype(BF16)
 
@@ -374,10 +382,9 @@
                 if r > CORES:
                     landed(0, h, side)
                 weights = weigh(gq[h], h, r)
-                landed(1, h, far)
                 if r > CORES:
                     landed(1, h, side)
-                back[h] = mix(*weights, h, r)
+                back[h] = mix(*weights, h, r, far, functools.partial(landed, 1, h, far))
             for h in range(moved):
                 give(h, other).wait_recv()
         for copy in sent:
@@ -418,7 +425,7 @@
             pltpu.VMEM((moved, local, dim), BF16),
             pltpu.VMEM((moved, local, dim), BF16),
             pltpu.VMEM((1, dim), F32),
-            pltpu.VMEM((heads, 8, dim), F32),
+            pltpu.VMEM((heads, 1, dim), F32),
             pltpu.SemaphoreType.DMA((4,)),
             pltpu.SemaphoreType.DMA((n,)),
             pltpu.SemaphoreType.DMA((n,)),

time: 12.2 us -> 12 us (0.984)
  the two profiles are of different devices: /device:TPU:21 before, /device:TPU:0 now
where the time goes in v5:
time: 12 us; the launch traced here: 11.9 us
  Pallas kernels  11.2 us (93%)
  between operations  0.66 us (6%)
    pallas_call x1, Pallas kernels, on_device(): pl.pallas_call(body, out_shape=pltpu.VMEM((heads, local, dim), BF16), in_...  10.3 us
    pallas_call x1, Pallas kernels, on_device(): pl.pallas_call(functools.partial(interleave, heads, local), out_shape=jax...  0.88 us

profile of v5, /device:TPU:0, one launch (start us, length us, event | category | flops | bytes accessed | tf_op | source)
XLA Modules:
  0.0 11.9 jit_solution(9246288301360482563)
XLA Ops:
  0.7 10.3 %shard_map.55.back_ref = bf16[4,128,128]{2,1,0:T(8,128)(2,1)S(1)} custom-call(f32[1]{0:T(128)S(6)} %copy.6.hw_ref, f32[1,128]{1,0:T(1,128)} %bitcast.8, bf16[512,128]{1,0:T(8,128)(2,1)} %bitcast.5, bf16[512,128]{1,0:T(8,128)(2,1)} %bitcast.6, bf16[512,128]{1,0:T(8,128)(2,1)} %bitcast.7), custom_call_target="tpu_custom_call" | custom-call | tf_op jit(solution)/shard_map/pallas_call | solution.py:450
  11.0 0.9 %shard_map.56 = bf16[512,128]{1,0:T(8,128)(2,1)} custom-call(bf16[4,128,128]{2,1,0:T(8,128)(2,1)S(1)} %shard_map.55.back_ref), custom_call_target="tpu_custom_call" | custom-call | tf_op jit(solution)/shard_map/pallas_call | solution.py:465
